TPU v7x, 32 devices: a whole 2x2x4 slice. The times are simulated.
32 devices in a mesh: ep: 8 (over z, x), tp: 4 (over y, core).
Axes of the slice: x: 2, y: 2, z: 4, core: 2. Of those that a mesh axis runs over, the one named last changes fastest.
Arguments:
- mix_values: bfloat16 [4096, 2048], P('ep', 'tp'), may hold values from -6 to 6
- mix_inner_gate: bfloat16 [4096, 2048], P('ep', 'tp'), may hold values from -6 to 6
- mix_outer_gate: bfloat16 [4096, 2048], P('ep', 'tp'), may hold values from -6 to 6
- conv_taps: bfloat16 [3, 2048], replicated, may hold values from -3 to 3
- mix_out_weight: bfloat16 [2048, 2048], P('tp'), may hold values from -0.125 to 0.125
- moe_input: bfloat16 [4096, 2048], P('ep'), may hold values from -36 to 36
- norm_gain: float32 [2048], replicated, may hold values from 0.1 to 1.9
- routes: int32 [4096, 2], P('ep'), may hold values from 0 to 7, all different within a row; in each aligned block of 128 rows (0 to 127, 128 to 255, ...) at most 64 rows name the same one
- route_weights: float32 [4096, 2], P('ep'), may hold values from 0.05 to 1
- expert_gate: bfloat16 [8, 2048, 1024], P('ep', None, 'tp'), may hold values from -0.125 to 0.125
- expert_up: bfloat16 [8, 2048, 1024], P('ep', None, 'tp'), may hold values from -0.125 to 0.125
- expert_down: bfloat16 [8, 1024, 2048], P('ep', 'tp'), may hold values from -0.1875 to 0.1875
- shared_gate: bfloat16 [2048, 1024], P(None, 'tp'), may hold values from -0.125 to 0.125
- shared_up: bfloat16 [2048, 1024], P(None, 'tp'), may hold values from -0.125 to 0.125
- shared_down: bfloat16 [1024, 2048], P('tp'), may hold values from -0.1875 to 0.1875
Outputs:
- mixed_out: bfloat16 [4096, 2048], P(('ep', 'tp'))
- expert_out: bfloat16 [4096, 2048], P(('ep', 'tp'))
Inputs may be any that keep to these rules, and one draw needn't show every extreme that they name: `routes`: each row names 2 different experts; in each aligned block of 128 rows no expert is named more than 64 times, and in every draw some block names some expert exactly 64 times.
All inputs are finite; a program needn't handle non-finite values.
Results may differ from a plain program's by a relative error of at most 0.012.
Values may be sent and summed in bfloat16 or wider, within the bound.
A program may use at most 128 MiB of HBM per device.

v0:
```python
import jax
import jax.numpy as jnp
from jax import lax
from jax.sharding import PartitionSpec as P


def from_behind(value, axis, steps):
    count = lax.axis_size(axis)
    initial, last = (max(0, -steps), min(count, count - steps))
    return lax.ppermute(value, axis, [(source, source + steps) for source in range(initial, last)])


def slot_table(route_block, experts, capacity):
    tokens, top = route_block.shape
    flat = route_block.reshape(-1)
    onehot = (flat[:, None] == jnp.arange(experts, dtype=jnp.int32)[None, :]).astype(jnp.int32)
    before = jnp.cumsum(onehot, axis=0) - onehot
    target = flat * capacity + jnp.sum(before * onehot, axis=1)
    match = target[None, :] == jnp.arange(experts * capacity, dtype=jnp.int32)[:, None]
    owner = jnp.sum(
        jnp.where(match, jnp.arange(tokens * top, dtype=jnp.int32)[None, :] // top, 0), axis=1
    )
    filled = jnp.any(match, axis=1)
    return (
        target.reshape(tokens, top),
        owner.reshape(experts, capacity),
        filled.reshape(experts, capacity),
    )


def dispatch(block_rows, owner, filled):
    return jnp.where(filled[:, :, None], block_rows[owner], jnp.zeros((), jnp.bfloat16))


def on_device(
    mix_values,
    mix_inner_gate,
    mix_outer_gate,
    conv_taps,
    mix_out_weight,
    moe_input,
    norm_gain,
    routes,
    route_weights,
    expert_gate,
    expert_up,
    expert_down,
    shared_gate,
    shared_up,
    shared_down,
):
    parts = lax.axis_size("tp")
    member = lax.axis_index("tp")
    groups = lax.axis_size("ep")
    rows_here, width_here = mix_values.shape
    reach = conv_taps.shape[0] - 1
    taps = lax.dynamic_slice_in_dim(conv_taps, member * width_here, width_here, 1).astype(
        jnp.float32
    )
    boundary = from_behind(
        jnp.stack([mix_values[rows_here - reach :], mix_inner_gate[rows_here - reach :]]), "ep", 1
    )
    product = jnp.concatenate(
        [
            boundary[1].astype(jnp.float32) * boundary[0].astype(jnp.float32),
            mix_inner_gate.astype(jnp.float32) * mix_values.astype(jnp.float32),
        ],
        axis=0,
    )
    convolved = taps[0] * product[0:rows_here]
    for offset in range(1, reach + 1):
        convolved = convolved + taps[offset] * product[offset : offset + rows_here]
    gated_rows = (mix_outer_gate.astype(jnp.float32) * convolved).astype(jnp.bfloat16)
    mixed = lax.psum_scatter(
        jnp.dot(gated_rows, mix_out_weight, preferred_element_type=jnp.float32).astype(
            jnp.bfloat16
        ),
        "tp",
        scatter_dimension=0,
        tiled=True,
    )
    local_experts = expert_gate.shape[0]
    experts = local_experts * groups
    width = moe_input.shape[1]
    block = moe_input.shape[0] // parts
    top = routes.shape[1]
    capacity = 2 * block * top // experts
    values = moe_input.astype(jnp.float32)
    scale = lax.rsqrt(jnp.mean(values * values, axis=1, keepdims=True) + 1e-06)
    normed_all = (values * scale * norm_gain).astype(jnp.bfloat16)
    own_weights = lax.dynamic_slice_in_dim(route_weights, member * block, block, 0)
    shared_gate_part = jnp.dot(normed_all, shared_gate, preferred_element_type=jnp.float32)
    shared_up_part = jnp.dot(normed_all, shared_up, preferred_element_type=jnp.float32)
    hidden_shared = (jax.nn.silu(shared_gate_part) * shared_up_part).astype(jnp.bfloat16)
    hidden_shared = hidden_shared.reshape(parts, block, hidden_shared.shape[1])
    own_routes = lax.dynamic_slice_in_dim(routes, member * block, block, 0)
    own_target, owner, filled = slot_table(own_routes, experts, capacity)
    own_rows = lax.dynamic_slice_in_dim(normed_all, member * block, block, 0)
    arrived = lax.all_to_all(
        dispatch(own_rows, owner, filled), "ep", split_axis=0, concat_axis=0, tiled=True
    )
    rows = lax.all_gather(
        arrived.reshape(1, groups, local_experts, capacity, width), "tp", axis=0, tiled=True
    )
    gate_part = jnp.einsum(
        "nsjcd,jdf->nsjcf", rows, expert_gate, preferred_element_type=jnp.float32
    )
    up_part = jnp.einsum("nsjcd,jdf->nsjcf", rows, expert_up, preferred_element_type=jnp.float32)
    hidden_routed = (jax.nn.silu(gate_part) * up_part).astype(jnp.bfloat16)
    routed_rows = groups * local_experts * capacity
    block_span = routed_rows + block
    number = block_span * lax.axis_size("tp") // block_span
    out_routed = jnp.einsum(
        "nsjcf,jfd->nsjcd", hidden_routed, expert_down, preferred_element_type=jnp.float32
    ).reshape(number, routed_rows, width)
    out_shared = jnp.einsum(
        "ntf,fd->ntd", hidden_shared, shared_down, preferred_element_type=jnp.float32
    )
    summed = lax.psum_scatter(
        jnp.concatenate([out_routed, out_shared], axis=1)
        .reshape(block_span * lax.axis_size("tp"), width)
        .astype(jnp.bfloat16),
        "tp",
        scatter_dimension=0,
        tiled=True,
    ).astype(jnp.float32)
    routed_back = (
        summed[:routed_rows].astype(jnp.bfloat16).reshape(groups, local_experts * capacity, width)
    )
    returned = lax.all_to_all(routed_back, "ep", split_axis=0, concat_axis=0, tiled=True).reshape(
        experts * capacity, width
    )
    chosen = returned[own_target]
    mix_weights = 2.5 * own_weights / jnp.sum(own_weights, axis=1, keepdims=True)
    total = summed[routed_rows:]
    for slot_number in range(top):
        total = total + mix_weights[:, slot_number : slot_number + 1] * chosen[
            :, slot_number
        ].astype(jnp.float32)
    expert_out = total.astype(jnp.bfloat16)
    return (mixed, expert_out)


def solution(mesh):
    return jax.shard_map(
        on_device,
        mesh=mesh,
        in_specs=(
            P("ep", "tp"),
            P("ep", "tp"),
            P("ep", "tp"),
            P(),
            P("tp", None),
            P("ep", None),
            P(),
            P("ep", None),
            P("ep", None),
            P("ep", None, "tp"),
            P("ep", None, "tp"),
            P("ep", "tp", None),
            P(None, "tp"),
            P(None, "tp"),
            P("tp", None),
        ),
        out_specs=(P(("ep", "tp"), None), P(("ep", "tp"), None)),
        check_vma=False,
    )
```

profile of v0, /device:TPU:0, one launch (start us, length us, event | category | flops | bytes accessed | tf_op | source)
XLA Modules:
  0.0 325.2 jit_solution(13791687452439275770)
XLA Ops:
  7.2 0.8 constant_dynamic-slice_fusion.2
  8.5 0.6 reduce-window.6
  9.9 2.2 fusion
  12.2 0.5 fusion.2
  12.7 1.4 copy-done.2
  14.2 3.3 %gather_fusion = bf16[512,2048]{1,0:T(8,128)(2,1)} fusion(bf16[128,2048]{1,0:T(8,128)(2,1)S(1)} %constant_dynamic-slice_fusion.1, s32[1024]{0:T(1024)S(1)} %pad_clamp_fusion.1), kind=kCustom, calls=%fused_computation | custom fusion | bytes 4196352 | tf_op jit(solution)/shard_map/gather | solution.py:32
  17.6 1.8 broadcast_select_fusion
  19.4 55.4 %all_to_all.10 = bf16[8,64,2048]{2,1,0:T(8,128)(2,1)} all-to-all(bf16[8,64,2048]{2,1,0:T(8,128)(2,1)S(1)} %broadcast_select_fusion), channel_id=1, replica_groups=mesh['ep'=8,'tp'=4] {'ep'}, dimensions={0} | all-to-all | bytes 4194304 | tf_op jit(solution)/shard_map/all_to_all | solution.py:99
  74.8 0.2 reduce-scatter.5.cloned.1.call-start
  75.1 2.7 fusion.39
  77.9 0.7 fusion.8
  78.6 0.5 copy-done.4
  79.1 2.0 convolution_convert_fusion.1
  81.1 51.2 %all-gather.3.cloned.1.call-done = bf16[32,64,2048]{2,1,0:T(8,128)(2,1)} async-done(((bf16[8,64,2048]{2,1,0:T(8,128)(2,1)}), bf16[32,64,2048]{2,1,0:T(8,128)(2,1)}) %all-gather.3.cloned.1.call-update) | async-done | bytes 8388624 | tf_op jit(solution)/shard_map/all_gather | solution.py:102
  132.3 7.4 %fusion.22 = f32[4,8,64,256]{3,2,1,0:T(8,128)} fusion(bf16[4,8,64,2048]{3,2,1,0:T(8,128)(2,1)} %bitcast.124, bf16[1,2048,256]{2,1,0:T(8,128)(2,1)} %param.24), kind=kOutput, calls=%fused_computation.39 | convolution fusion | flops 2147483648 | bytes 11534336 | tf_op jit(solution)/shard_map/nsjcd,jdf->nsjcf/dot_general | solution.py:105
  139.6 13.8 %convolution_convert_fusion = bf16[4,8,64,2048]{3,2,1,0:T(8,128)(2,1)} fusion(bf16[1,256,2048]{2,1,0:T(8,128)(2,1)} %param.26, bf16[4,8,64,2048]{3,2,1,0:T(8,128)(2,1)} %bitcast.125, f32[4,8,64,256]{3,2,1,0:T(8,128)} %fusion.22, bf16[1,2048,256]{2,1,0:T(8,128)(2,1)} %param.25), kind=kOutput, calls=%fused_computation.3 | convolution fusion | flops 4302307328 | bytes 20971520 | tf_op jit(solution)/shard_map/nsjcf,jfd->nsjcd/dot_general | solution.py:113
  153.5 12.2 %pad_maximum_fusion = bf16[4,640,2048]{2,1,0:T(8,128)(2,1)} fusion(bf16[4,128,2048]{2,1,0:T(8,128)(2,1)} %convolution_convert_fusion.1, bf16[4,512,2048]{2,1,0:T(8,128)(2,1)} %bitcast.118), kind=kLoop, calls=%fused_computation.2 | loop fusion | flops 20971520 | bytes 20971520 | tf_op jit(solution)/shard_map/concatenate | solution.py:120
  165.7 1.0 copy-done.5
  166.9 3.4 %collective-permute-start = (bf16[2,2,512]{2,1,0:T(2,128)(2,1)S(1)}, bf16[2,2,512]{2,1,0:T(2,128)(2,1)S(1)}, u32[]{:S(2)}, u32[]{:S(2)}) collective-permute-start(bf16[2,2,512]{2,1,0:T(2,128)(2,1)S(1)} %pad_maximum_fusion.2), channel_id=1, source_target_pairs={{0,4},{4,8},{8,12},{12,16},{16,20},{20,24},{24,28},{1,5},{5,9},{9,... | collective-permute-start | bytes 12296 | tf_op jit(solution)/shard_map/ppermute | solution.py:10
  170.3 0.7 dynamic-slice_convert_fusion
  171.0 1.1 convert_multiply_fusion.4
  172.1 78.1 %reduce-scatter.5.cloned.1.call-done = bf16[640,2048]{1,0:T(8,128)(2,1)} async-done(((bf16[2560,2048]{1,0:T(8,128)(2,1)}), bf16[640,2048]{1,0:T(8,128)(2,1)}) %reduce-scatter.5.cloned.1.call-update) | async-done | bytes 2621456 | tf_op jit(solution)/shard_map/reduce_scatter | solution.py:119
  250.2 3.2 slice.86
  253.4 5.6 %all-to-all-start.1 = ((bf16[8,64,2048]{2,1,0:T(8,128)(2,1)}), bf16[8,64,2048]{2,1,0:T(8,128)(2,1)}, u32[]{:S(2)}, u32[]{:S(2)}) async-start(bf16[8,64,2048]{2,1,0:T(8,128)(2,1)} %bitcast.119), calls=%async_computation.3 | async-start | bytes 4194304 | tf_op jit(solution)/shard_map/all_to_all | solution.py:130
  259.0 0.3 reduce-scatter.3.cloned.1.call-start
  259.4 4.8 %convolution_convert_fusion.2 = bf16[512,2048]{1,0:T(8,128)(2,1)} fusion(bf16[512,2048]{1,0:T(8,128)(2,1)S(1)} %copy-done, f32[2,512]{1,0:T(2,128)S(1)} %multiply_bitcast_fusion, f32[512,512]{1,0:T(8,128)} %convert_multiply_fusion.4, bf16[512,512]{1,0:T(8,128)(2,1)S(1)} %copy-done.10, f32[512]{0:T(512)S(1)} %bitcast.122, f32[512]{0:T(512)S(1)} %bitcast.123, ...), kind=kOutput, calls=%fused_computation.10 | convolution fusion | flops 1077411840 | bytes 5777408 | tf_op jit(solution)/shard_map/dot_general | solution.py:75
  264.5 0.4 copy-done.8
  264.9 42.3 %all-to-all-done.1 = bf16[8,64,2048]{2,1,0:T(8,128)(2,1)} async-done(((bf16[8,64,2048]{2,1,0:T(8,128)(2,1)}), bf16[8,64,2048]{2,1,0:T(8,128)(2,1)}, u32[]{:S(2)}, u32[]{:S(2)}) %all-to-all-start.1) | async-done | bytes 2097184 | tf_op jit(solution)/shard_map/all_to_all | solution.py:130
  307.2 5.2 %gather_fusion.1 = bf16[256,2048]{1,0:T(8,128)(2,1)} fusion(bf16[512,2048]{1,0:T(8,128)(2,1)} %bitcast.37, s32[1024]{0:T(1024)S(1)} %pad_clamp_fusion), kind=kCustom, calls=%fused_computation.1 | custom fusion | bytes 2098176 | tf_op jit(solution)/shard_map/gather | solution.py:133
  312.4 1.7 reshape.182
  314.2 1.5 fusion.37
  315.7 3.0 fusion.17
  (53 shorter events, 2.1 us)
Async XLA Ops:
  7.2 252.2 %copy-start = (bf16[512,2048]{1,0:T(8,128)(2,1)S(1)}, bf16[512,2048]{1,0:T(8,128)(2,1)}, u32[]{:S(2)}) copy-start(bf16[512,2048]{1,0:T(8,128)(2,1)} %param.19) | copy-start | bytes 6291460
  7.2 5.0 %copy-start.7 = (f32[2048]{0:T(1024)S(1)}, f32[2048]{0:T(1024)}, u32[]{:S(2)}) copy-start(f32[2048]{0:T(1024)} %param.21) | copy-start | bytes 24580
  7.2 125.1 %all-gather.3.cloned.1.call-start = ((), (), s32[]{:S(2)}) async-start(), calls=%async_computation.6 | async-start | bytes 10485760 | tf_op jit(solution)/shard_map/all_gather | solution.py:102
  9.9 2.3 copy-start.1
  12.7 1.4 copy-start.2
  74.8 175.4 %reduce-scatter.5.cloned.1.call-start = ((), (), s32[]{:S(2)}) async-start(), calls=%async_computation.5 | async-start | bytes 13107200 | tf_op jit(solution)/shard_map/reduce_scatter | solution.py:119
  75.1 2.7 copy-start.3
  75.1 2.8 copy-start.9
  77.9 1.2 copy-start.4
  165.6 1.0 copy-start.5
  165.6 1.2 copy-start.6
  166.9 92.4 %collective-permute-start = (bf16[2,2,512]{2,1,0:T(2,128)(2,1)S(1)}, bf16[2,2,512]{2,1,0:T(2,128)(2,1)S(1)}, u32[]{:S(2)}, u32[]{:S(2)}) collective-permute-start(bf16[2,2,512]{2,1,0:T(2,128)(2,1)S(1)} %pad_maximum_fusion.2), channel_id=1, source_target_pairs={{0,4},{4,8},{8,12},{12,16},{16,20},{20,24},{24,28},{1,5},{5,9},{9,... | collective-permute-start | bytes 12296 | tf_op jit(solution)/shard_map/ppermute | solution.py:10
  253.4 5.9 %copy-start.10 = (bf16[512,512]{1,0:T(8,128)(2,1)S(1)}, bf16[512,512]{1,0:T(8,128)(2,1)}, u32[]{:S(2)}) copy-start(bf16[512,512]{1,0:T(8,128)(2,1)} %param.17) | copy-start | bytes 1572868
  253.4 53.8 %all-to-all-start.1 = ((bf16[8,64,2048]{2,1,0:T(8,128)(2,1)}), bf16[8,64,2048]{2,1,0:T(8,128)(2,1)}, u32[]{:S(2)}, u32[]{:S(2)}) async-start(bf16[8,64,2048]{2,1,0:T(8,128)(2,1)} %bitcast.119), calls=%async_computation.3 | async-start | bytes 4194304 | tf_op jit(solution)/shard_map/all_to_all | solution.py:130
  259.0 59.6 %reduce-scatter.3.cloned.1.call-start = ((), (), s32[]{:S(2)}) async-start(), calls=%async_computation.4 | async-start | bytes 2621440 | tf_op jit(solution)/shard_map/reduce_scatter | solution.py:74
  264.2 0.7 copy-start.8
Sparse Core Ops, SparseCore 0:
  74.9 57.2 all-gather.2
  165.8 84.3 reduce-scatter.4
  264.3 31.3 reduce-scatter.2
where the time goes:
time: 326 us; the launch traced here: 325 us
  waiting for transfers between devices  172 us (53%)
  blocking collectives  55.4 us (17%)
  matrix products  31.4 us (10%)
  other arithmetic  22.7 us (7%)
  local copies, waits for them, and re-layouts  20.4 us (6%)
  between operations  14 us (4%)
  starting transfers between devices  9.53 us (3%)
    reduce_scatter x1, waiting for transfers between devices, on_device(): lax.psum_scatter(jnp.concatenate([out_routed, out_shared], axis=1).reshap...  78.1 us
    all_to_all x1, blocking collectives, on_device(): lax.all_to_all(dispatch(own_rows, owner, filled), 'ep', split_axis=0, con...  55.4 us
    all_gather x1, waiting for transfers between devices, on_device(): lax.all_gather(arrived.reshape(1, groups, local_experts, capacity, width)...  51.2 us
    all_to_all x1, waiting for transfers between devices, on_device(): lax.all_to_all(routed_back, 'ep', split_axis=0, concat_axis=0, tiled=True)  42.3 us
    dot_general x1, matrix products, on_device(): jnp.einsum('nsjcf,jfd->nsjcd', hidden_routed, expert_down, preferred_elem...  13.8 us
    concatenate x1, other arithmetic, on_device(): jnp.concatenate([out_routed, out_shared], axis=1)  12.2 us
    dot_general x1, matrix products, on_device(): jnp.einsum('nsjcd,jdf->nsjcf', rows, expert_gate, preferred_element_type=...  7.36 us
    gather x2, local copies, waits for them, and re-layouts, on_device(): chosen = returned[own_target]  6.94 us
  transfers between devices with their start and end apart: 5, of which 3 were waited for; matrix products, arithmetic and copies ran while one was open for 8% of the time, Pallas kernels for 0%

commit v1 on v0

v1 whole, which is shorter than its diff:
```python
import jax
import jax.numpy as jnp
from jax import lax
from jax.sharding import PartitionSpec as P


def from_behind(value, axis, steps):
    count = lax.axis_size(axis)
    initial, last = (max(0, -steps), min(count, count - steps))
    return lax.ppermute(value, axis, [(source, source + steps) for source in range(initial, last)])


def normalized(rows, gain):
    values = rows.astype(jnp.float32)
    scale = lax.rsqrt(jnp.mean(values * values, axis=1, keepdims=True) + 1e-06)
    return (values * scale * gain).astype(jnp.bfloat16)


def slot_targets(route_block, experts, capacity):
    tokens, top = route_block.shape
    names = jnp.arange(experts, dtype=jnp.int32)[None, :]
    named = [route_block[:, k : k + 1] == names for k in range(top)]
    any_named = named[0]
    for k in range(1, top):
        any_named = any_named | named[k]
    earlier = (
        jnp.arange(tokens, dtype=jnp.int32)[:, None] > jnp.arange(tokens, dtype=jnp.int32)[None, :]
    )
    before = jnp.dot(
        earlier.astype(jnp.bfloat16),
        any_named.astype(jnp.bfloat16),
        preferred_element_type=jnp.float32,
    ).astype(jnp.int32)
    return [
        route_block[:, k : k + 1] * capacity
        + jnp.sum(jnp.where(named[k], before, 0), axis=1, keepdims=True)
        for k in range(top)
    ]


def on_device(
    mix_values,
    mix_inner_gate,
    mix_outer_gate,
    conv_taps,
    mix_out_weight,
    moe_input,
    norm_gain,
    routes,
    route_weights,
    expert_gate,
    expert_up,
    expert_down,
    shared_gate,
    shared_up,
    shared_down,
):
    parts = lax.axis_size("tp")
    member = lax.axis_index("tp")
    groups = lax.axis_size("ep")
    rows_here, width_here = mix_values.shape
    reach = conv_taps.shape[0] - 1
    taps = lax.dynamic_slice_in_dim(conv_taps, member * width_here, width_here, 1).astype(
        jnp.float32
    )
    boundary = from_behind(
        jnp.stack([mix_values[rows_here - reach :], mix_inner_gate[rows_here - reach :]]), "ep", 1
    )
    product = jnp.concatenate(
        [
            boundary[1].astype(jnp.float32) * boundary[0].astype(jnp.float32),
            mix_inner_gate.astype(jnp.float32) * mix_values.astype(jnp.float32),
        ],
        axis=0,
    )
    convolved = taps[0] * product[0:rows_here]
    for offset in range(1, reach + 1):
        convolved = convolved + taps[offset] * product[offset : offset + rows_here]
    gated_rows = (mix_outer_gate.astype(jnp.float32) * convolved).astype(jnp.bfloat16)
    mixed = lax.psum_scatter(
        jnp.dot(gated_rows, mix_out_weight, preferred_element_type=jnp.float32).astype(
            jnp.bfloat16
        ),
        "tp",
        scatter_dimension=0,
        tiled=True,
    )
    local_experts = expert_gate.shape[0]
    experts = local_experts * groups
    width = moe_input.shape[1]
    block = moe_input.shape[0] // parts
    top = routes.shape[1]
    capacity = 2 * block * top // experts
    whole_gate = lax.all_gather(expert_gate, "tp", axis=0)
    whole_up = lax.all_gather(expert_up, "tp", axis=0)
    whole_down = lax.all_gather(expert_down, "tp", axis=0)

    own_rows = normalized(
        lax.dynamic_slice_in_dim(moe_input, member * block, block, 0), norm_gain
    )
    own_routes = lax.dynamic_slice_in_dim(routes, member * block, block, 0)
    targets = slot_targets(own_routes, experts, capacity)
    slots = jnp.arange(experts * capacity, dtype=jnp.int32)[None, :]
    picks = [(target == slots).astype(jnp.bfloat16) for target in targets]
    placed = picks[0]
    for k in range(1, top):
        placed = placed + picks[k]
    sent = lax.dot_general(
        placed, own_rows, (((0,), (0,)), ((), ())), preferred_element_type=jnp.float32
    ).astype(jnp.bfloat16)
    arrived = lax.all_to_all(
        sent.reshape(groups, local_experts * capacity, width),
        "ep",
        split_axis=0,
        concat_axis=0,
        tiled=True,
    ).reshape(groups, local_experts, capacity, width)

    normed_all = normalized(moe_input, norm_gain)
    shared_gate_part = jnp.dot(normed_all, shared_gate, preferred_element_type=jnp.float32)
    shared_up_part = jnp.dot(normed_all, shared_up, preferred_element_type=jnp.float32)
    hidden_shared = (jax.nn.silu(shared_gate_part) * shared_up_part).astype(jnp.bfloat16)
    shared = lax.psum_scatter(
        jnp.dot(hidden_shared, shared_down, preferred_element_type=jnp.float32).astype(
            jnp.bfloat16
        ),
        "tp",
        scatter_dimension=0,
        tiled=True,
    ).astype(jnp.float32)

    finished = []
    for expert in range(local_experts):
        rows = arrived[:, expert].reshape(groups * capacity, width)
        hidden = []
        for part in range(parts):
            gate_part = jnp.dot(
                rows, whole_gate[part, expert], preferred_element_type=jnp.float32
            )
            up_part = jnp.dot(rows, whole_up[part, expert], preferred_element_type=jnp.float32)
            hidden.append((jax.nn.silu(gate_part) * up_part).astype(jnp.bfloat16))
        down = whole_down[:, expert].reshape(-1, width)
        finished.append(
            jnp.dot(
                jnp.concatenate(hidden, axis=1), down, preferred_element_type=jnp.float32
            )
            .astype(jnp.bfloat16)
            .reshape(groups, 1, capacity, width)
        )
    routed_back = finished[0] if local_experts == 1 else jnp.concatenate(finished, axis=1)
    returned = lax.all_to_all(
        routed_back.reshape(groups, local_experts * capacity, width),
        "ep",
        split_axis=0,
        concat_axis=0,
        tiled=True,
    ).reshape(experts * capacity, width)
    own_weights = lax.dynamic_slice_in_dim(route_weights, member * block, block, 0)
    mix_weights = 2.5 * own_weights / jnp.sum(own_weights, axis=1, keepdims=True)
    total = shared
    for k in range(top):
        chosen = jnp.dot(picks[k], returned, preferred_element_type=jnp.float32)
        total = total + mix_weights[:, k : k + 1] * chosen
    expert_out = total.astype(jnp.bfloat16)
    return (mixed, expert_out)


def solution(mesh):
    return jax.shard_map(
        on_device,
        mesh=mesh,
        in_specs=(
            P("ep", "tp"),
            P("ep", "tp"),
            P("ep", "tp"),
            P(),
            P("tp", None),
            P("ep", None),
            P(),
            P("ep", None),
            P("ep", None),
            P("ep", None, "tp"),
            P("ep", None, "tp"),
            P("ep", "tp", None),
            P(None, "tp"),
            P(None, "tp"),
            P("tp", None),
        ),
        out_specs=(P(("ep", "tp"), None), P(("ep", "tp"), None)),
        check_vma=False,
    )
```

time: 326 us -> 194 us (0.60)
  waiting for transfers between devices: 172 us -> 103 us
  blocking collectives: 55.4 us -> 0 us
  matrix products: 31.4 us -> 51.5 us
  local copies, waits for them, and re-layouts: 20.4 us -> 2.82 us
  other arithmetic: 22.7 us -> 5.43 us
  starting transfers between devices: 9.53 us -> 16.8 us
    reduce_scatter x1, waiting for transfers between devices: 78.1 us -> 17.4 us  [on_device(): lax.psum_scatter(jnp.dot(hidden_shared, shared_down, preferred_element_ty...]
    all_to_all x1 -> x0, blocking collectives: 55.4 us -> none  [on_device(): lax.all_to_all(dispatch(own_rows, owner, filled), 'ep', split_axis=0, con...]
    all_gather x1 -> x3, waiting for transfers between devices: 51.2 us -> 22.7 us  [the longest x1 22.7 us: on_device(): whole_down = lax.all_gather(expert_down, 'tp', axis=0)]
    dot_general x4 -> x14, matrix products: 23.9 us -> 45.7 us  [the longest x4 12.9 us: on_device(): jnp.dot(rows, whole_gate[part, expert], preferred_element_type=jnp.float32)]
    all_to_all x1 -> x2, waiting for transfers between devices: 42.3 us -> 58 us  [the longest x1 31.2 us: on_device(): lax.all_to_all(sent.reshape(groups, local_experts * capacity, width), 'ep...]
    concatenate x1 -> x0, other arithmetic: 12.2 us -> none  [on_device(): jnp.concatenate([out_routed, out_shared], axis=1)]
    gather x3 -> x0, local copies, waits for them, and re-layouts: 10.3 us -> none  [the longest x2 6.94 us: on_device(): chosen = returned[own_target]]
    all_to_all x1 -> x2, starting transfers between devices: 5.64 us -> 12.8 us  [the longest x1 7.28 us: on_device(): lax.all_to_all(sent.reshape(groups, local_experts * capacity, width), 'ep...]
  transfers between devices with their start and end apart: 5 -> 8, of which waited for: 3 -> 6; matrix products, arithmetic and copies ran while one was open for 8% -> 30% of each run, Pallas kernels for 0% -> 0%
where the time goes in v1:
time: 194 us; the launch traced here: 193 us
  waiting for transfers between devices  103 us (53%)
  matrix products  51.5 us (27%)
  starting transfers between devices  16.8 us (9%)
  between operations  13.9 us (7%)
  other arithmetic  5.43 us (3%)
  local copies, waits for them, and re-layouts  2.82 us (1%)
    all_to_all x1, waiting for transfers between devices, on_device(): lax.all_to_all(sent.reshape(groups, local_experts * capacity, width), 'ep...  31.2 us
    all_to_all x1, waiting for transfers between devices, on_device(): lax.all_to_all(routed_back.reshape(groups, local_experts * capacity, widt...  26.8 us
    all_gather x1, waiting for transfers between devices, on_device(): whole_down = lax.all_gather(expert_down, 'tp', axis=0)  22.7 us
    reduce_scatter x1, waiting for transfers between devices, on_device(): lax.psum_scatter(jnp.dot(hidden_shared, shared_down, preferred_element_ty...  17.4 us
    dot_general x4, matrix products, on_device(): jnp.dot(rows, whole_gate[part, expert], preferred_element_type=jnp.float32)  12.9 us
    dot_general x4, matrix products, on_device(): jnp.dot(rows, whole_up[part, expert], preferred_element_type=jnp.float32)  12.4 us
    all_to_all x1, starting transfers between devices, on_device(): lax.all_to_all(sent.reshape(groups, local_experts * capacity, width), 'ep...  7.28 us
    dot_general x1, matrix products, on_device(): jnp.dot(jnp.concatenate(hidden, axis=1), down, preferred_element_type=jnp...  6.12 us
  transfers between devices with their start and end apart: 8, of which 6 were waited for; matrix products, arithmetic and copies ran while one was open for 30% of the time, Pallas kernels for 0%

profile of v1, /device:TPU:0, one launch (start us, length us, event | category | flops | bytes accessed | tf_op | source)
XLA Modules:
  0.0 193.2 jit_solution(7441418015061131727)
XLA Ops:
  7.2 0.7 all-gather.7.cloned.1.call-update
  8.0 0.7 all-gather.9.cloned.1.call-update
  8.7 0.7 all-gather.11.cloned.1.call-update
  9.4 1.2 fusion.17
  10.6 0.7 constant_dynamic-slice_fusion
  11.5 3.2 %convolution_convert_fusion.1 = bf16[512,2048]{1,0:T(8,128)(2,1)} fusion(f32[2048]{0:T(1024)S(1)} %copy-done.2, f32[128]{0:T(128)S(1)} %add_rsqrt_fusion.1, bf16[512,2048]{1,0:T(8,128)(2,1)} %param.20, s32[]{:T(128)S(6)} %select_n.16, s32[128]{0:T(128)S(1)} %get-tuple-element.10, s32[128]{0:T(128)S(1)} %get-tuple-element.9), kind=kOutput, calls=%fused_computation.6 | convolution fusion | flops 271056896 | bytes 2631172 | tf_op jit(solution)/shard_map/dot_general | solution.py:108
  14.8 7.3 %all-to-all-start = ((bf16[8,64,2048]{2,1,0:T(8,128)(2,1)}), bf16[8,64,2048]{2,1,0:T(8,128)(2,1)}, u32[]{:S(2)}, u32[]{:S(2)}) async-start(bf16[8,64,2048]{2,1,0:T(8,128)(2,1)} %bitcast.73), calls=%async_computation.2 | async-start | bytes 4194304 | tf_op jit(solution)/shard_map/all_to_all | solution.py:111
  22.1 0.9 slice_bitcast_fusion.16
  23.0 3.9 %collective-permute-start = (bf16[2,2,512]{2,1,0:T(2,128)(2,1)S(1)}, bf16[2,2,512]{2,1,0:T(2,128)(2,1)S(1)}, u32[]{:S(2)}, u32[]{:S(2)}) collective-permute-start(bf16[2,2,512]{2,1,0:T(2,128)(2,1)S(1)} %pad_maximum_fusion.1), channel_id=1, source_target_pairs={{0,4},{4,8},{8,12},{12,16},{16,20},{20,24},{24,28},{1,5},{5,9},{9,... | collective-permute-start | bytes 12296 | tf_op jit(solution)/shard_map/ppermute | solution.py:10
  26.9 2.1 %fusion = f32[512]{0:T(512)S(1)} fusion(bf16[512,2048]{1,0:T(8,128)(2,1)} %param.20), kind=kLoop, calls=%fused_computation.2 | loop fusion | flops 3145216 | bytes 2099200 | tf_op jit(solution)/shard_map/reduce_sum | solution.py:15
  29.0 2.0 %fusion.34 = f32[512,256]{1,0:T(8,128)S(1)} fusion(bf16[2048,256]{1,0:T(8,128)(2,1)} %param.27, bf16[512,2048]{1,0:T(8,128)(2,1)S(1)} %copy-done.1, f32[2048]{0:T(1024)S(1)} %copy-done.2, f32[512]{0:T(512)S(1)} %add_rsqrt_fusion), kind=kOutput, calls=%fused_computation.60 | convolution fusion | flops 541065216 | bytes 3680256 | tf_op jit(solution)/shard_map/dot_general | solution.py:120
  31.0 5.9 %convolution_convert_fusion.2 = bf16[512,2048]{1,0:T(8,128)(2,1)} fusion(bf16[256,2048]{1,0:T(8,128)(2,1)} %param.29, bf16[2048,256]{1,0:T(8,128)(2,1)} %param.28, bf16[512,2048]{1,0:T(8,128)(2,1)} %param.20, f32[2048]{0:T(1024)S(1)} %copy-done.2, f32[512]{0:T(512)S(1)} %add_rsqrt_fusion, f32[512,256]{1,0:T(8,128)S(1)} %fusion.34), kind=kOutput, calls=%fused_computation.7 | convolution fusion | flops 1079771136 | bytes 6825984 | tf_op jit(solution)/shard_map/dot_general | solution.py:124
  36.9 0.7 dynamic-slice_convert_fusion
  37.6 1.4 convert_multiply_fusion.4
  39.2 31.2 %all-to-all-done = bf16[8,64,2048]{2,1,0:T(8,128)(2,1)} async-done(((bf16[8,64,2048]{2,1,0:T(8,128)(2,1)}), bf16[8,64,2048]{2,1,0:T(8,128)(2,1)}, u32[]{:S(2)}, u32[]{:S(2)}) %all-to-all-start) | async-done | bytes 2097184 | tf_op jit(solution)/shard_map/all_to_all | solution.py:111
  70.4 3.6 %fusion.20 = f32[512,256]{1,0:T(8,128)} fusion(bf16[512,2048]{1,0:T(8,128)(2,1)} %bitcast.14, bf16[4,2048,256]{2,1,0:T(8,128)(2,1)} %all-gather.7.cloned.1.call-done), kind=kOutput, calls=%fused_computation.40 | convolution fusion | flops 536870912 | bytes 3670016 | tf_op jit(solution)/shard_map/dot_general | solution.py:137
  73.9 3.1 %fusion.23 = f32[512,256]{1,0:T(8,128)} fusion(bf16[512,2048]{1,0:T(8,128)(2,1)} %bitcast.14, bf16[4,2048,256]{2,1,0:T(8,128)(2,1)S(1)} %copy-done.5), kind=kOutput, calls=%fused_computation.49 | convolution fusion | flops 536870912 | bytes 3670016 | tf_op jit(solution)/shard_map/dot_general | solution.py:137
  77.1 3.1 %fusion.22 = f32[512,256]{1,0:T(8,128)} fusion(bf16[512,2048]{1,0:T(8,128)(2,1)} %bitcast.14, bf16[4,2048,256]{2,1,0:T(8,128)(2,1)S(1)} %copy-done.5), kind=kOutput, calls=%fused_computation.46 | convolution fusion | flops 536870912 | bytes 3670016 | tf_op jit(solution)/shard_map/dot_general | solution.py:137
  80.2 3.1 %fusion.21 = f32[512,256]{1,0:T(8,128)} fusion(bf16[512,2048]{1,0:T(8,128)(2,1)} %bitcast.14, bf16[4,2048,256]{2,1,0:T(8,128)(2,1)S(1)} %copy-done.5), kind=kOutput, calls=%fused_computation.43 | convolution fusion | flops 536870912 | bytes 3670016 | tf_op jit(solution)/shard_map/dot_general | solution.py:137
  83.3 2.8 %fusion.10 = bf16[512,256]{1,0:T(8,128)(2,1)S(1)} fusion(bf16[512,2048]{1,0:T(8,128)(2,1)} %bitcast.14, bf16[4,2048,256]{2,1,0:T(8,128)(2,1)} %all-gather.9.cloned.1.call-done, f32[512,256]{1,0:T(8,128)} %fusion.20), kind=kOutput, calls=%fused_computation.25 | convolution fusion | flops 537657344 | bytes 3932160 | tf_op jit(solution)/shard_map/dot_general | solution.py:140
  86.7 3.1 %fusion.7 = bf16[512,256]{1,0:T(8,128)(2,1)} fusion(bf16[512,2048]{1,0:T(8,128)(2,1)} %bitcast.14, bf16[4,2048,256]{2,1,0:T(8,128)(2,1)S(1)} %copy-done.4, f32[512,256]{1,0:T(8,128)S(1)} %copy-done.8), kind=kOutput, calls=%fused_computation.22 | convolution fusion | flops 537657344 | bytes 3932160 | tf_op jit(solution)/shard_map/dot_general | solution.py:140
  89.7 3.3 %fusion.8 = bf16[512,256]{1,0:T(8,128)(2,1)} fusion(bf16[512,2048]{1,0:T(8,128)(2,1)} %bitcast.14, bf16[4,2048,256]{2,1,0:T(8,128)(2,1)S(1)} %copy-done.4, f32[512,256]{1,0:T(8,128)S(1)} %copy-done.7), kind=kOutput, calls=%fused_computation.23 | convolution fusion | flops 537657344 | bytes 3932160 | tf_op jit(solution)/shard_map/dot_general | solution.py:140
  93.0 3.2 %fusion.9 = bf16[512,256]{1,0:T(8,128)(2,1)} fusion(bf16[512,2048]{1,0:T(8,128)(2,1)} %bitcast.14, bf16[4,2048,256]{2,1,0:T(8,128)(2,1)S(1)} %copy-done.4, f32[512,256]{1,0:T(8,128)S(1)} %copy-done.6), kind=kOutput, calls=%fused_computation.24 | convolution fusion | flops 537657344 | bytes 3932160 | tf_op jit(solution)/shard_map/dot_general | solution.py:140
  96.2 22.7 %all-gather.11.cloned.1.call-done = bf16[4,256,2048]{2,1,0:T(8,128)(2,1)} async-done(((bf16[1,256,2048]{2,1,0:T(8,128)(2,1)}), bf16[4,256,2048]{2,1,0:T(8,128)(2,1)}) %all-gather.11.cloned.1.call-update) | async-done | bytes 4194320 | tf_op jit(solution)/shard_map/all_gather | solution.py:96
  118.9 6.1 %convolution_convert_fusion = bf16[512,2048]{1,0:T(8,128)(2,1)} fusion(bf16[1024,2048]{1,0:T(8,128)(2,1)} %bitcast.78, bf16[512,256]{1,0:T(8,128)(2,1)S(1)} %fusion.10, bf16[512,256]{1,0:T(8,128)(2,1)} %fusion.9, bf16[512,256]{1,0:T(8,128)(2,1)} %fusion.8, bf16[512,256]{1,0:T(8,128)(2,1)} %fusion.7), kind=kOutput, calls=%fused_computation.5 | convolution fusion | flops 2152726528 | bytes 7340032 | tf_op jit(solution)/shard_map/dot_general | solution.py:144
  125.0 5.5 %all-to-all-start.1 = ((bf16[8,64,2048]{2,1,0:T(8,128)(2,1)}), bf16[8,64,2048]{2,1,0:T(8,128)(2,1)}, u32[]{:S(2)}, u32[]{:S(2)}) async-start(bf16[8,64,2048]{2,1,0:T(8,128)(2,1)} %bitcast.74), calls=%async_computation.3 | async-start | bytes 4194304 | tf_op jit(solution)/shard_map/all_to_all | solution.py:151
  130.6 3.8 %convolution_convert_fusion.3 = bf16[512,2048]{1,0:T(8,128)(2,1)} fusion(bf16[512,2048]{1,0:T(8,128)(2,1)S(1)} %copy-done, f32[2,512]{1,0:T(2,128)S(1)} %multiply_bitcast_fusion, f32[512,512]{1,0:T(8,128)S(1)} %convert_multiply_fusion.4, bf16[512,512]{1,0:T(8,128)(2,1)} %param.17, f32[512]{0:T(512)S(1)} %bitcast.76, f32[512]{0:T(512)S(1)} %bitcast.77, ...), kind=kOutput, calls=%fused_computation.8 | convolution fusion | flops 1077411840 | bytes 5777408 | tf_op jit(solution)/shard_map/dot_general | solution.py:81
  135.1 17.4 %reduce-scatter.5.cloned.1.call-done = bf16[128,2048]{1,0:T(8,128)(2,1)} async-done(((bf16[512,2048]{1,0:T(8,128)(2,1)}), bf16[128,2048]{1,0:T(8,128)(2,1)}) %reduce-scatter.5.cloned.1.call-update) | async-done | bytes 524304 | tf_op jit(solution)/shard_map/reduce_scatter | solution.py:123
  152.5 26.8 %all-to-all-done.1 = bf16[8,64,2048]{2,1,0:T(8,128)(2,1)} async-done(((bf16[8,64,2048]{2,1,0:T(8,128)(2,1)}), bf16[8,64,2048]{2,1,0:T(8,128)(2,1)}, u32[]{:S(2)}, u32[]{:S(2)}) %all-to-all-start.1) | async-done | bytes 2097184 | tf_op jit(solution)/shard_map/all_to_all | solution.py:151
  179.3 2.2 %fusion.4 = f32[128,2048]{1,0:T(8,128)S(1)} fusion(bf16[512,2048]{1,0:T(8,128)(2,1)} %bitcast.25, bf16[128,2048]{1,0:T(8,128)(2,1)} %reduce-scatter.5.cloned.1.call-done, f32[128]{0:T(128)S(1)} %get-tuple-element.8, s32[128]{0:T(128)S(1)} %get-tuple-element.9), kind=kOutput, calls=%fused_computation.12 | convolution fusion | flops 269287424 | bytes 3671040 | tf_op jit(solution)/shard_map/dot_general | solution.py:162
  181.4 2.9 %fusion.5 = bf16[128,2048]{1,0:T(8,128)(2,1)} fusion(f32[128,2048]{1,0:T(8,128)S(1)} %fusion.4, bf16[512,2048]{1,0:T(8,128)(2,1)} %bitcast.25, f32[128]{0:T(128)S(1)} %get-tuple-element.7, s32[128]{0:T(128)S(1)} %get-tuple-element.10), kind=kOutput, calls=%fused_computation.13 | convolution fusion | flops 269287424 | bytes 3671040 | tf_op jit(solution)/shard_map/dot_general | solution.py:162
  184.3 2.3 %reduce-scatter.3.cloned.1.call-done = bf16[128,2048]{1,0:T(8,128)(2,1)} async-done(((bf16[512,2048]{1,0:T(8,128)(2,1)}), bf16[128,2048]{1,0:T(8,128)(2,1)}) %reduce-scatter.3.cloned.1.call-update) | async-done | bytes 524304 | tf_op jit(solution)/shard_map/reduce_scatter | solution.py:80
  (39 shorter events, 1.9 us)
Async XLA Ops:
  7.2 123.4 %copy-start = (bf16[512,2048]{1,0:T(8,128)(2,1)S(1)}, bf16[512,2048]{1,0:T(8,128)(2,1)}, u32[]{:S(2)}) copy-start(bf16[512,2048]{1,0:T(8,128)(2,1)} %param.19) | copy-start | bytes 6291460
  7.2 4.3 %copy-start.2 = (f32[2048]{0:T(1024)S(1)}, f32[2048]{0:T(1024)}, u32[]{:S(2)}) copy-start(f32[2048]{0:T(1024)} %param.21) | copy-start | bytes 24580
  7.2 63.2 %all-gather.7.cloned.1.call-start = ((), (), s32[]{:S(2)}) async-start(), calls=%async_computation.6 | async-start | bytes 5242880 | tf_op jit(solution)/shard_map/all_gather | solution.py:94
  7.9 75.3 %all-gather.9.cloned.1.call-start = ((), (), s32[]{:S(2)}) async-start(), calls=%async_computation.7 | async-start | bytes 5242880 | tf_op jit(solution)/shard_map/all_gather | solution.py:95
  8.7 110.2 %all-gather.11.cloned.1.call-start = ((), (), s32[]{:S(2)}) async-start(), calls=%async_computation.8 | async-start | bytes 5242880 | tf_op jit(solution)/shard_map/all_gather | solution.py:96
  14.8 55.6 %all-to-all-start = ((bf16[8,64,2048]{2,1,0:T(8,128)(2,1)}), bf16[8,64,2048]{2,1,0:T(8,128)(2,1)}, u32[]{:S(2)}, u32[]{:S(2)}) async-start(bf16[8,64,2048]{2,1,0:T(8,128)(2,1)} %bitcast.73), calls=%async_computation.2 | async-start | bytes 4194304 | tf_op jit(solution)/shard_map/all_to_all | solution.py:111
  22.0 130.4 %reduce-scatter.5.cloned.1.call-start = ((), (), s32[]{:S(2)}) async-start(), calls=%async_computation.5 | async-start | bytes 2621440 | tf_op jit(solution)/shard_map/reduce_scatter | solution.py:123
  22.1 6.9 %copy-start.1 = (bf16[512,2048]{1,0:T(8,128)(2,1)S(1)}, bf16[512,2048]{1,0:T(8,128)(2,1)}, u32[]{:S(2)}) copy-start(bf16[512,2048]{1,0:T(8,128)(2,1)} %param.20) | copy-start | bytes 6291460
  23.0 16.2 %collective-permute-start = (bf16[2,2,512]{2,1,0:T(2,128)(2,1)S(1)}, bf16[2,2,512]{2,1,0:T(2,128)(2,1)S(1)}, u32[]{:S(2)}, u32[]{:S(2)}) collective-permute-start(bf16[2,2,512]{2,1,0:T(2,128)(2,1)S(1)} %pad_maximum_fusion.1), channel_id=1, source_target_pairs={{0,4},{4,8},{8,12},{12,16},{16,20},{20,24},{24,28},{1,5},{5,9},{9,... | collective-permute-start | bytes 12296 | tf_op jit(solution)/shard_map/ppermute | solution.py:10
  70.4 3.6 %copy-start.5 = (bf16[4,2048,256]{2,1,0:T(8,128)(2,1)S(1)}, bf16[4,2048,256]{2,1,0:T(8,128)(2,1)}, u32[]{:S(2)}) copy-start(bf16[4,2048,256]{2,1,0:T(8,128)(2,1)} %all-gather.7.cloned.1.call-done) | copy-start | bytes 12582916
  83.2 3.3 %copy-start.4 = (bf16[4,2048,256]{2,1,0:T(8,128)(2,1)S(1)}, bf16[4,2048,256]{2,1,0:T(8,128)(2,1)}, u32[]{:S(2)}) copy-start(bf16[4,2048,256]{2,1,0:T(8,128)(2,1)} %all-gather.9.cloned.1.call-done) | copy-start | bytes 12582916
  83.3 3.4 %copy-start.8 = (f32[512,256]{1,0:T(8,128)S(1)}, f32[512,256]{1,0:T(8,128)}, u32[]{:S(2)}) copy-start(f32[512,256]{1,0:T(8,128)} %fusion.23) | copy-start | bytes 1572868
  86.7 3.1 %copy-start.7 = (f32[512,256]{1,0:T(8,128)S(1)}, f32[512,256]{1,0:T(8,128)}, u32[]{:S(2)}) copy-start(f32[512,256]{1,0:T(8,128)} %fusion.22) | copy-start | bytes 1572868
  89.7 3.3 %copy-start.6 = (f32[512,256]{1,0:T(8,128)S(1)}, f32[512,256]{1,0:T(8,128)}, u32[]{:S(2)}) copy-start(f32[512,256]{1,0:T(8,128)} %fusion.21) | copy-start | bytes 1572868
  125.0 54.3 %all-to-all-start.1 = ((bf16[8,64,2048]{2,1,0:T(8,128)(2,1)}), bf16[8,64,2048]{2,1,0:T(8,128)(2,1)}, u32[]{:S(2)}, u32[]{:S(2)}) async-start(bf16[8,64,2048]{2,1,0:T(8,128)(2,1)} %bitcast.74), calls=%async_computation.3 | async-start | bytes 4194304 | tf_op jit(solution)/shard_map/all_to_all | solution.py:151
  130.5 56.1 %reduce-scatter.3.cloned.1.call-start = ((), (), s32[]{:S(2)}) async-start(), calls=%async_computation.4 | async-start | bytes 2621440 | tf_op jit(solution)/shard_map/reduce_scatter | solution.py:80
  134.4 0.7 copy-start.3
Sparse Core Ops, SparseCore 0:
  9.6 37.1 all-gather.6
  48.3 34.4 all-gather.8
  84.4 34.4 all-gather.10
  121.3 31.1 reduce-scatter.4
  155.4 31.1 reduce-scatter.2

commit v2 on v1

--- a/solution.py
+++ b/solution.py
@@ -8,6 +8,43 @@
     count = lax.axis_size(axis)
     initial, last = (max(0, -steps), min(count, count - steps))
     return lax.ppermute(value, axis, [(source, source + steps) for source in range(initial, last)])
+
+
+def across(value, axis, stride):
+    count = lax.axis_size(axis)
+    return lax.ppermute(value, axis, [(source, source ^ stride) for source in range(count)])
+
+
+def gathered_parts(shard, axis):
+    count = lax.axis_size(axis)
+    if count & (count - 1):
+        whole = lax.all_gather(shard, axis, axis=0)
+        return [whole[part] for part in range(count)]
+    held = [shard]
+    stride = count // 2
+    while stride:
+        held = [piece for value in held for piece in (value, across(value, axis, stride))]
+        stride //= 2
+    return held
+
+
+def scattered_sum(rows, axis):
+    count = lax.axis_size(axis)
+    if count & (count - 1):
+        return lax.psum_scatter(rows, axis, scatter_dimension=0, tiled=True).astype(jnp.float32)
+    here = lax.axis_index(axis)
+    block = rows.shape[0] // count
+    held = rows.reshape((count, block) + rows.shape[1:])
+    stride = 1
+    while stride < count:
+        bit = (here // stride) % 2
+        pairs = held.reshape((held.shape[0] // 2, 2) + held.shape[1:])
+        kept = lax.dynamic_index_in_dim(pairs, bit, 1, keepdims=False)
+        given = lax.dynamic_index_in_dim(pairs, 1 - bit, 1, keepdims=False)
+        got = across(given.astype(jnp.bfloat16), axis, stride)
+        held = kept.astype(jnp.float32) + got.astype(jnp.float32)
+        stride *= 2
+    return held.reshape((block,) + rows.shape[1:]).astype(jnp.float32)
 
 
 def normalized(rows, gain):
@@ -66,34 +103,17 @@
     boundary = from_behind(
         jnp.stack([mix_values[rows_here - reach :], mix_inner_gate[rows_here - reach :]]), "ep", 1
     )
-    product = jnp.concatenate(
-        [
-            boundary[1].astype(jnp.float32) * boundary[0].astype(jnp.float32),
-            mix_inner_gate.astype(jnp.float32) * mix_values.astype(jnp.float32),
-        ],
-        axis=0,
-    )
-    convolved = taps[0] * product[0:rows_here]
-    for offset in range(1, reach + 1):
-        convolved = convolved + taps[offset] * product[offset : offset + rows_here]
-    gated_rows = (mix_outer_gate.astype(jnp.float32) * convolved).astype(jnp.bfloat16)
-    mixed = lax.psum_scatter(
-        jnp.dot(gated_rows, mix_out_weight, preferred_element_type=jnp.float32).astype(
-            jnp.bfloat16
-        ),
-        "tp",
-        scatter_dimension=0,
-        tiled=True,
-    )
     local_experts = expert_gate.shape[0]
     experts = local_experts * groups
     width = moe_input.shape[1]
     block = moe_input.shape[0] // parts
     top = routes.shape[1]
     capacity = 2 * block * top // experts
-    whole_gate = lax.all_gather(expert_gate, "tp", axis=0)
-    whole_up = lax.all_gather(expert_up, "tp", axis=0)
-    whole_down = lax.all_gather(expert_down, "tp", axis=0)
+    gate_parts = gathered_parts(expert_gate, "tp")
+    up_parts = gathered_parts(expert_up, "tp")
+    down_parts = gathered_parts(expert_down, "tp")
+    whole_gate = lax.optimization_barrier(jnp.concatenate(gate_parts, axis=2))
+    whole_up = lax.optimization_barrier(jnp.concatenate(up_parts, axis=2))
 
     own_rows = normalized(
         lax.dynamic_slice_in_dim(moe_input, member * block, block, 0), norm_gain
@@ -108,6 +128,7 @@
     sent = lax.dot_general(
         placed, own_rows, (((0,), (0,)), ((), ())), preferred_element_type=jnp.float32
     ).astype(jnp.bfloat16)
+    sent, boundary = lax.optimization_barrier((sent, boundary))
     arrived = lax.all_to_all(
         sent.reshape(groups, local_experts * capacity, width),
         "ep",
@@ -116,37 +137,49 @@
         tiled=True,
     ).reshape(groups, local_experts, capacity, width)
 
+    product = jnp.concatenate(
+        [
+            boundary[1].astype(jnp.float32) * boundary[0].astype(jnp.float32),
+            mix_inner_gate.astype(jnp.float32) * mix_values.astype(jnp.float32),
+        ],
+        axis=0,
+    )
+    convolved = taps[0] * product[0:rows_here]
+    for offset in range(1, reach + 1):
+        convolved = convolved + taps[offset] * product[offset : offset + rows_here]
+    gated_rows = (mix_outer_gate.astype(jnp.float32) * convolved).astype(jnp.bfloat16)
+    mixed_part = jnp.dot(
+        gated_rows, mix_out_weight, preferred_element_type=jnp.float32
+    ).astype(jnp.bfloat16)
+    mixed = scattered_sum(mixed_part, "tp").astype(jnp.bfloat16)
+
     normed_all = normalized(moe_input, norm_gain)
     shared_gate_part = jnp.dot(normed_all, shared_gate, preferred_element_type=jnp.float32)
     shared_up_part = jnp.dot(normed_all, shared_up, preferred_element_type=jnp.float32)
     hidden_shared = (jax.nn.silu(shared_gate_part) * shared_up_part).astype(jnp.bfloat16)
-    shared = lax.psum_scatter(
-        jnp.dot(hidden_shared, shared_down, preferred_element_type=jnp.float32).astype(
-            jnp.bfloat16
-        ),
-        "tp",
-        scatter_dimension=0,
-        tiled=True,
-    ).astype(jnp.float32)
+    shared_part = jnp.dot(
+        hidden_shared, shared_down, preferred_element_type=jnp.float32
+    ).astype(jnp.bfloat16)
+    shared = scattered_sum(shared_part, "tp")
 
     finished = []
     for expert in range(local_experts):
         rows = arrived[:, expert].reshape(groups * capacity, width)
-        hidden = []
-        for part in range(parts):
-            gate_part = jnp.dot(
-                rows, whole_gate[part, expert], preferred_element_type=jnp.float32
+        gate_part = jnp.dot(rows, whole_gate[expert], preferred_element_type=jnp.float32)
+        up_part = jnp.dot(rows, whole_up[expert], preferred_element_type=jnp.float32)
+        hidden = (jax.nn.silu(gate_part) * up_part).astype(jnp.bfloat16)
+        part_width = hidden.shape[1] // parts
+        result = jnp.zeros((), jnp.float32)
+        span = max(1, parts // 2)
+        for start in range(0, parts, span):
+            result = result + jnp.dot(
+                hidden[:, start * part_width : (start + span) * part_width],
+                jnp.concatenate(
+                    [piece[expert] for piece in down_parts[start : start + span]], axis=0
+                ),
+                preferred_element_type=jnp.float32,
             )
-            up_part = jnp.dot(rows, whole_up[part, expert], preferred_element_type=jnp.float32)
-            hidden.append((jax.nn.silu(gate_part) * up_part).astype(jnp.bfloat16))
-        down = whole_down[:, expert].reshape(-1, width)
-        finished.append(
-            jnp.dot(
-                jnp.concatenate(hidden, axis=1), down, preferred_element_type=jnp.float32
-            )
-            .astype(jnp.bfloat16)
-            .reshape(groups, 1, capacity, width)
-        )
+        finished.append(result.astype(jnp.bfloat16).reshape(groups, 1, capacity, width))
     routed_back = finished[0] if local_experts == 1 else jnp.concatenate(finished, axis=1)
     returned = lax.all_to_all(
         routed_back.reshape(groups, local_experts * capacity, width),

time: 194 us -> 171 us (0.88)
  waiting for transfers between devices: 103 us -> 86.2 us
  matrix products: 51.5 us -> 35.3 us
  between operations: 13.9 us -> 0.93 us
  other arithmetic: 5.43 us -> 17 us
  starting transfers between devices: 16.8 us -> 22.9 us
  local copies, waits for them, and re-layouts: 2.82 us -> 7.82 us
    ppermute x0 -> x13, waiting for transfers between devices: none -> 68.6 us  [across(): lax.ppermute(value, axis, [(source, source ^ stride) for source in range(...]
    all_to_all x1, waiting for transfers between devices: 31.2 us -> 0.01 us  [on_device(): lax.all_to_all(sent.reshape(groups, local_experts * capacity, width), 'ep...]
    all_gather x3 -> x0, waiting for transfers between devices: 22.7 us -> none  [the longest x1 22.7 us: on_device(): whole_down = lax.all_gather(expert_down, 'tp', axis=0)]
    reduce_scatter x2 -> x0, waiting for transfers between devices: 19.7 us -> none  [the longest x1 17.4 us: on_device(): lax.psum_scatter(jnp.dot(hidden_shared, shared_down, preferred_element_ty...]
    dot_general x9 -> x4, matrix products: 31.4 us -> 16.1 us  [the longest x2 6.62 us: on_device(): jnp.dot(hidden[:, start * part_width:(start + span) * part_width], jnp.co...]
    all_to_all x1, waiting for transfers between devices: 26.8 us -> 17.6 us  [on_device(): lax.all_to_all(routed_back.reshape(groups, local_experts * capacity, widt...]
    concatenate x0 -> x2, other arithmetic: none -> 7.58 us  [the longest x1 3.82 us: on_device(): whole_up = lax.optimization_barrier(jnp.concatenate(up_parts, axis=2))]
    ppermute x0 -> x13, starting transfers between devices: none -> 7.31 us  [across(): lax.ppermute(value, axis, [(source, source ^ stride) for source in range(...]
  transfers between devices with their start and end apart: 8 -> 16, of which waited for: 6 -> 5; matrix products, arithmetic and copies ran while one was open for 30% -> 30% of each run, Pallas kernels for 0% -> 0%
where the time goes in v2:
time: 171 us; the launch traced here: 170 us
  waiting for transfers between devices  86.2 us (50%)
  matrix products  35.3 us (21%)
  starting transfers between devices  22.9 us (13%)
  other arithmetic  17 us (10%)
  local copies, waits for them, and re-layouts  7.82 us (5%)
    ppermute x13, waiting for transfers between devices, across(): lax.ppermute(value, axis, [(source, source ^ stride) for source in range(...  68.6 us
    all_to_all x1, waiting for transfers between devices, on_device(): lax.all_to_all(routed_back.reshape(groups, local_experts * capacity, widt...  17.6 us
    ppermute x13, starting transfers between devices, across(): lax.ppermute(value, axis, [(source, source ^ stride) for source in range(...  7.31 us
    dot_general x2, matrix products, on_device(): jnp.dot(hidden[:, start * part_width:(start + span) * part_width], jnp.co...  6.62 us
    all_to_all x1, starting transfers between devices, on_device(): lax.all_to_all(routed_back.reshape(groups, local_experts * capacity, widt...  5.85 us
    dot_general x1, matrix products, on_device(): jnp.dot(hidden_shared, shared_down, preferred_element_type=jnp.float32)  5.69 us
    dot_general x1, matrix products, on_device(): jnp.dot(rows, whole_gate[expert], preferred_element_type=jnp.float32)  5.3 us
    all_to_all x1, starting transfers between devices, on_device(): lax.all_to_all(sent.reshape(groups, local_experts * capacity, width), 'ep...  4.88 us
  transfers between devices with their start and end apart: 16, of which 5 were waited for; matrix products, arithmetic and copies ran while one was open for 30% of the time, Pallas kernels for 0%

profile of v2, /device:TPU:0, one launch (start us, length us, event | category | flops | bytes accessed | tf_op | source)
XLA Modules:
  0.0 170.2 jit_solution(10480597474333010152)
XLA Ops:
  1.5 4.9 %collective-permute-start = (bf16[2,2,512]{2,1,0:T(2,128)(2,1)S(1)}, bf16[2,2,512]{2,1,0:T(2,128)(2,1)S(1)}, u32[]{:S(2)}, u32[]{:S(2)}) collective-permute-start(bf16[2,2,512]{2,1,0:T(2,128)(2,1)S(1)} %pad_maximum_fusion.3), channel_id=1, source_target_pairs={{0,4},{4,8},{8,12},{12,16},{16,20},{20,24},{24,28},{1,5},{5,9},{9,... | collective-permute-start | bytes 12296 | tf_op jit(solution)/shard_map/ppermute | solution.py:10
  7.1 1.2 fusion.21
  8.5 3.2 %convolution_convert_fusion.1 = bf16[512,2048]{1,0:T(8,128)(2,1)} fusion(f32[2048]{0:T(1024)} %param.21, f32[128]{0:T(128)S(1)} %add_rsqrt_fusion.1, bf16[512,2048]{1,0:T(8,128)(2,1)} %param.20, s32[]{:T(128)S(6)} %select_n.56, s32[128]{0:T(128)S(1)} %get-tuple-element.14, s32[128]{0:T(128)S(1)} %get-tuple-element.13), kind=kOutput, calls=%fused_computation.13 | convolution fusion | flops 271056896 | bytes 2631172 | tf_op jit(solution)/shard_map/dot_general | solution.py:128
  11.8 4.9 %all-to-all-start = ((bf16[8,64,2048]{2,1,0:T(8,128)(2,1)}), bf16[8,64,2048]{2,1,0:T(8,128)(2,1)}, u32[]{:S(2)}, u32[]{:S(2)}) async-start(bf16[8,64,2048]{2,1,0:T(8,128)(2,1)} %bitcast.78), calls=%async_computation | async-start | bytes 4194304 | tf_op jit(solution)/shard_map/all_to_all | solution.py:132
  16.7 1.5 collective-permute-start.6
  19.2 1.5 collective-permute-start.12
  21.6 2.4 %convert_multiply_fusion.4 = f32[512,512]{1,0:T(8,128)} fusion(bf16[512,512]{1,0:T(8,128)(2,1)} %param.15, bf16[512,512]{1,0:T(8,128)(2,1)} %param.16), kind=kLoop, calls=%fused_computation.53 | loop fusion | flops 786432 | bytes 2097152 | tf_op jit(solution)/shard_map/mul | solution.py:143
  23.9 19.1 %collective-permute-done.6 = bf16[1,2048,256]{2,1,0:T(8,128)(2,1)} collective-permute-done((bf16[1,2048,256]{2,1,0:T(8,128)(2,1)}, bf16[1,2048,256]{2,1,0:T(8,128)(2,1)}, u32[]{:S(2)}, u32[]{:S(2)}) %collective-permute-start.6) | collective-permute-done | bytes 1048608 | tf_op jit(solution)/shard_map/ppermute | solution.py:15
  43.5 22.0 %collective-permute-done.9 = bf16[1,2048,256]{2,1,0:T(8,128)(2,1)} collective-permute-done((bf16[1,2048,256]{2,1,0:T(8,128)(2,1)}, bf16[1,2048,256]{2,1,0:T(8,128)(2,1)}, u32[]{:S(2)}, u32[]{:S(2)}) %collective-permute-start.9) | collective-permute-done | bytes 1048608 | tf_op jit(solution)/shard_map/ppermute | solution.py:15
  65.5 3.4 %fusion.29 = f32[512,256]{1,0:T(8,128)} fusion(bf16[2048,256]{1,0:T(8,128)(2,1)} %param.27, bf16[512,2048]{1,0:T(8,128)(2,1)} %param.20, f32[2048]{0:T(1024)S(1)} %copy-done.8, f32[512]{0:T(512)S(1)} %add_rsqrt_fusion), kind=kOutput, calls=%fused_computation.54 | convolution fusion | flops 541065216 | bytes 3680256 | tf_op jit(solution)/shard_map/dot_general | solution.py:157
  69.5 16.7 %collective-permute-done.12 = bf16[1,256,2048]{2,1,0:T(8,128)(2,1)S(1)} collective-permute-done((bf16[1,256,2048]{2,1,0:T(8,128)(2,1)}, bf16[1,256,2048]{2,1,0:T(8,128)(2,1)S(1)}, u32[]{:S(2)}, u32[]{:S(2)}) %collective-permute-start.12) | collective-permute-done | bytes 1048608 | tf_op jit(solution)/shard_map/ppermute | solution.py:15
  86.2 3.8 %pad_maximum_fusion = bf16[1,2048,1024]{2,1,0:T(8,128)(2,1)} fusion(bf16[1,2048,256]{2,1,0:T(8,128)(2,1)} %collective-permute-done.7, bf16[1,2048,256]{2,1,0:T(8,128)(2,1)} %collective-permute-done.6, bf16[1,2048,256]{2,1,0:T(8,128)(2,1)} %collective-permute-done.5, bf16[1,2048,256]{2,1,0:T(8,128)(2,1)} %param.24), kind=kLoop, calls=%fused_computation.5 | loop fusion | flops 16777216 | bytes 8388608 | tf_op jit(solution)/shard_map/concatenate | solution.py:115
  89.9 3.8 %pad_maximum_fusion.1 = bf16[1,2048,1024]{2,1,0:T(8,128)(2,1)} fusion(bf16[1,2048,256]{2,1,0:T(8,128)(2,1)} %collective-permute-done.10, bf16[1,2048,256]{2,1,0:T(8,128)(2,1)} %collective-permute-done.9, bf16[1,2048,256]{2,1,0:T(8,128)(2,1)} %collective-permute-done.8, bf16[1,2048,256]{2,1,0:T(8,128)(2,1)} %param.25), kind=kLoop, calls=%fused_computation.6 | loop fusion | flops 16777216 | bytes 8388608 | tf_op jit(solution)/shard_map/concatenate | solution.py:116
  93.8 5.3 %fusion.5 = f32[512,1024]{1,0:T(8,128)S(1)} fusion(bf16[512,2048]{1,0:T(8,128)(2,1)} %bitcast.22, bf16[1,2048,1024]{2,1,0:T(8,128)(2,1)} %pad_maximum_fusion), kind=kOutput, calls=%fused_computation.9 | convolution fusion | flops 2147483648 | bytes 8388608 | tf_op jit(solution)/shard_map/dot_general | solution.py:168
  99.1 4.1 %multiply_convert_fusion = bf16[512,1024]{1,0:T(8,128)(2,1)S(1)} fusion(f32[512,1024]{1,0:T(8,128)S(1)} %fusion.5, bf16[512,2048]{1,0:T(8,128)(2,1)} %bitcast.22, bf16[1,2048,1024]{2,1,0:T(8,128)(2,1)S(1)} %copy-done.4), kind=kOutput, calls=%fused_computation.26 | convolution fusion | flops 2150629376 | bytes 9437184 | tf_op jit(solution)/shard_map/dot_general | solution.py:169
  103.2 2.8 %fusion.7 = f32[512,2048]{1,0:T(8,128)S(1)} fusion(bf16[256,2048]{1,0:T(8,128)(2,1)} %bitcast.26, bf16[256,2048]{1,0:T(8,128)(2,1)} %bitcast.25, bf16[512,1024]{1,0:T(8,128)(2,1)S(1)} %multiply_convert_fusion), kind=kOutput, calls=%fused_computation.17 | convolution fusion | flops 1077936128 | bytes 6815744 | tf_op jit(solution)/shard_map/dot_general | solution.py:175
  106.0 3.8 %add_convert_fusion = bf16[512,2048]{1,0:T(8,128)(2,1)} fusion(f32[512,2048]{1,0:T(8,128)S(1)} %fusion.7, bf16[256,2048]{1,0:T(8,128)(2,1)} %bitcast.28, bf16[256,2048]{1,0:T(8,128)(2,1)S(1)} %bitcast.83, bf16[512,1024]{1,0:T(8,128)(2,1)S(1)} %multiply_convert_fusion), kind=kOutput, calls=%fused_computation.11 | convolution fusion | flops 1080033280 | bytes 8912896 | tf_op jit(solution)/shard_map/dot_general | solution.py:175
  109.9 5.9 %all-to-all-start.1 = ((bf16[8,64,2048]{2,1,0:T(8,128)(2,1)}), bf16[8,64,2048]{2,1,0:T(8,128)(2,1)}, u32[]{:S(2)}, u32[]{:S(2)}) async-start(bf16[8,64,2048]{2,1,0:T(8,128)(2,1)} %bitcast.77), calls=%async_computation.1 | async-start | bytes 4194304 | tf_op jit(solution)/shard_map/all_to_all | solution.py:184
  115.7 2.5 %convolution_convert_fusion.2 = bf16[512,2048]{1,0:T(8,128)(2,1)S(1)} fusion(bf16[512,2048]{1,0:T(8,128)(2,1)S(1)} %copy-done, f32[2,512]{1,0:T(2,128)S(1)} %multiply_bitcast_fusion, f32[512,512]{1,0:T(8,128)S(1)} %copy-done.7, bf16[512,512]{1,0:T(8,128)(2,1)} %param.17, f32[512]{0:T(512)S(1)} %bitcast.85, f32[512]{0:T(512)S(1)} %bitcast.86, ...), kind=kOutput, calls=%fused_computation.14 | convolution fusion | flops 1077411840 | bytes 5777408 | tf_op jit(solution)/shard_map/dot_general | solution.py:151
  118.2 1.3 copy-done.6
  119.5 1.1 dynamic-slice_bitcast_fusion.1
  120.8 5.7 %convolution_convert_fusion = bf16[512,2048]{1,0:T(8,128)(2,1)} fusion(bf16[256,2048]{1,0:T(8,128)(2,1)S(1)} %copy-done.10, bf16[2048,256]{1,0:T(8,128)(2,1)} %param.28, bf16[512,2048]{1,0:T(8,128)(2,1)} %param.20, f32[2048]{0:T(1024)S(1)} %copy-done.8, f32[512]{0:T(512)S(1)} %add_rsqrt_fusion, f32[512,256]{1,0:T(8,128)} %fusion.29), kind=kOutput, calls=%fused_computation.12 | convolution fusion | flops 1079771136 | bytes 6825984 | tf_op jit(solution)/shard_map/dot_general | solution.py:160
  126.5 2.3 %dynamic-slice_bitcast_fusion = bf16[2,128,2048]{2,1,0:T(8,128)(2,1)} fusion(bf16[2,2,128,2048]{3,2,1,0:T(8,128)(2,1)} %bitcast.79, s32[]{:T(128)S(6)} %select_n.61), kind=kLoop, calls=%fused_computation.49 | loop fusion | bytes 2097156 | tf_op jit(solution)/shard_map/jit(dynamic_index_in_dim)/squeeze | solution.py:43
  129.3 2.0 %convert_add_fusion.1 = f32[2,128,2048]{2,1,0:T(8,128)S(1)} fusion(bf16[2,128,2048]{2,1,0:T(8,128)(2,1)} %collective-permute-done.1, bf16[2,2,128,2048]{3,2,1,0:T(8,128)(2,1)} %bitcast.82, s32[]{:T(128)S(6)} %select_n.60), kind=kLoop, calls=%fused_computation.25 | loop fusion | flops 1572864 | bytes 4194308 | tf_op jit(solution)/shard_map/add | solution.py:45
  131.4 1.6 collective-permute-start.2
  133.3 1.3 copy-done.1
  135.3 10.9 %collective-permute-done.2 = bf16[1,128,2048]{2,1,0:T(8,128)(2,1)S(1)} collective-permute-done((bf16[1,128,2048]{2,1,0:T(8,128)(2,1)S(1)}, bf16[1,128,2048]{2,1,0:T(8,128)(2,1)S(1)}, u32[]{:S(2)}, u32[]{:S(2)}) %collective-permute-start.2) | collective-permute-done | bytes 524320 | tf_op jit(solution)/shard_map/ppermute | solution.py:15
  146.3 0.9 fusion.31
  147.2 17.6 %all-to-all-done.1 = bf16[8,64,2048]{2,1,0:T(8,128)(2,1)} async-done(((bf16[8,64,2048]{2,1,0:T(8,128)(2,1)}), bf16[8,64,2048]{2,1,0:T(8,128)(2,1)}, u32[]{:S(2)}, u32[]{:S(2)}) %all-to-all-start.1) | async-done | bytes 2097184 | tf_op jit(solution)/shard_map/all_to_all | solution.py:184
  164.7 2.1 %convolution_multiply_fusion.1 = f32[128,2048]{1,0:T(8,128)S(1)} fusion(bf16[512,2048]{1,0:T(8,128)(2,1)} %bitcast.30, f32[128]{0:T(128)S(1)} %get-tuple-element.11, s32[128]{0:T(128)S(1)} %get-tuple-element.13), kind=kOutput, calls=%fused_computation.16 | convolution fusion | flops 268763136 | bytes 3146752 | tf_op jit(solution)/shard_map/dot_general | solution.py:195
  166.8 2.2 %convolution_multiply_fusion = f32[128,2048]{1,0:T(8,128)S(1)} fusion(bf16[512,2048]{1,0:T(8,128)(2,1)} %bitcast.30, f32[128]{0:T(128)S(1)} %get-tuple-element.12, s32[128]{0:T(128)S(1)} %get-tuple-element.14), kind=kOutput, calls=%fused_computation.15 | convolution fusion | flops 268763136 | bytes 3146752 | tf_op jit(solution)/shard_map/dot_general | solution.py:195
  169.1 1.1 fusion.26
  (59 shorter events, 6.4 us)
Async XLA Ops:
  0.6 115.1 %copy-start = (bf16[512,2048]{1,0:T(8,128)(2,1)S(1)}, bf16[512,2048]{1,0:T(8,128)(2,1)}, u32[]{:S(2)}) copy-start(bf16[512,2048]{1,0:T(8,128)(2,1)} %param.19) | copy-start | bytes 6291460
  1.5 10.2 %collective-permute-start = (bf16[2,2,512]{2,1,0:T(2,128)(2,1)S(1)}, bf16[2,2,512]{2,1,0:T(2,128)(2,1)S(1)}, u32[]{:S(2)}, u32[]{:S(2)}) collective-permute-start(bf16[2,2,512]{2,1,0:T(2,128)(2,1)S(1)} %pad_maximum_fusion.3), channel_id=1, source_target_pairs={{0,4},{4,8},{8,12},{12,16},{16,20},{20,24},{24,28},{1,5},{5,9},{9,... | collective-permute-start | bytes 12296 | tf_op jit(solution)/shard_map/ppermute | solution.py:10
  11.8 82.0 %all-to-all-start = ((bf16[8,64,2048]{2,1,0:T(8,128)(2,1)}), bf16[8,64,2048]{2,1,0:T(8,128)(2,1)}, u32[]{:S(2)}, u32[]{:S(2)}) async-start(bf16[8,64,2048]{2,1,0:T(8,128)(2,1)} %bitcast.78), calls=%async_computation | async-start | bytes 4194304 | tf_op jit(solution)/shard_map/all_to_all | solution.py:132
  16.7 26.3 %collective-permute-start.6 = (bf16[1,2048,256]{2,1,0:T(8,128)(2,1)}, bf16[1,2048,256]{2,1,0:T(8,128)(2,1)}, u32[]{:S(2)}, u32[]{:S(2)}) collective-permute-start(bf16[1,2048,256]{2,1,0:T(8,128)(2,1)} %param.24), channel_id=1, source_target_pairs={{0,2},{1,3},{2,0},{3,1},{4,6},{5,7},{6,4},{7,5},{8,10},{9,11},{10,... | collective-permute-start | bytes 3145736 | tf_op jit(solution)/shard_map/ppermute | solution.py:15
  18.2 47.3 %collective-permute-start.9 = (bf16[1,2048,256]{2,1,0:T(8,128)(2,1)}, bf16[1,2048,256]{2,1,0:T(8,128)(2,1)}, u32[]{:S(2)}, u32[]{:S(2)}) collective-permute-start(bf16[1,2048,256]{2,1,0:T(8,128)(2,1)} %param.25), channel_id=1, source_target_pairs={{0,2},{1,3},{2,0},{3,1},{4,6},{5,7},{6,4},{7,5},{8,10},{9,11},{10,... | collective-permute-start | bytes 3145736 | tf_op jit(solution)/shard_map/ppermute | solution.py:15
  18.7 50.2 %collective-permute-start.5 = (bf16[1,2048,256]{2,1,0:T(8,128)(2,1)}, bf16[1,2048,256]{2,1,0:T(8,128)(2,1)}, u32[]{:S(2)}, u32[]{:S(2)}) collective-permute-start(bf16[1,2048,256]{2,1,0:T(8,128)(2,1)} %param.24), channel_id=1, source_target_pairs={{0,1},{1,0},{2,3},{3,2},{4,5},{5,4},{6,7},{7,6},{8,9},{9,8},{10,11... | collective-permute-start | bytes 3145736 | tf_op jit(solution)/shard_map/ppermute | solution.py:15
  18.7 71.2 %collective-permute-start.8 = (bf16[1,2048,256]{2,1,0:T(8,128)(2,1)}, bf16[1,2048,256]{2,1,0:T(8,128)(2,1)}, u32[]{:S(2)}, u32[]{:S(2)}) collective-permute-start(bf16[1,2048,256]{2,1,0:T(8,128)(2,1)} %param.25), channel_id=1, source_target_pairs={{0,1},{1,0},{2,3},{3,2},{4,5},{5,4},{6,7},{7,6},{8,9},{9,8},{10,11... | collective-permute-start | bytes 3145736 | tf_op jit(solution)/shard_map/ppermute | solution.py:15
  19.2 67.0 %collective-permute-start.12 = (bf16[1,256,2048]{2,1,0:T(8,128)(2,1)}, bf16[1,256,2048]{2,1,0:T(8,128)(2,1)S(1)}, u32[]{:S(2)}, u32[]{:S(2)}) collective-permute-start(bf16[1,256,2048]{2,1,0:T(8,128)(2,1)} %param.26), channel_id=1, source_target_pairs={{0,2},{1,3},{2,0},{3,1},{4,6},{5,7},{6,4},{7,5},{8,10},{9,11},{10,... | collective-permute-start | bytes 3145736 | tf_op jit(solution)/shard_map/ppermute | solution.py:15
  20.7 22.3 %copy-start.3 = (bf16[512,2048]{1,0:T(8,128)(2,1)S(1)}, bf16[512,2048]{1,0:T(8,128)(2,1)}, u32[]{:S(2)}) copy-start(bf16[512,2048]{1,0:T(8,128)(2,1)} %param.20) | copy-start | bytes 6291460
  21.6 43.9 %copy-start.8 = (f32[2048]{0:T(1024)S(1)}, f32[2048]{0:T(1024)}, u32[]{:S(2)}) copy-start(f32[2048]{0:T(1024)} %param.21) | copy-start | bytes 24580
  43.0 43.2 %collective-permute-start.7 = (bf16[1,2048,256]{2,1,0:T(8,128)(2,1)}, bf16[1,2048,256]{2,1,0:T(8,128)(2,1)}, u32[]{:S(2)}, u32[]{:S(2)}) collective-permute-start(bf16[1,2048,256]{2,1,0:T(8,128)(2,1)} %collective-permute-done.6), channel_id=1, source_target_pairs={{0,1},{1,0},{2,3},{3,2},{4,5},{5,4},{6,7},{7,6},{8,9},{9,8},{10,11... | collective-permute-start | bytes 3145736 | tf_op jit(solution)/shard_map/ppermute | solution.py:15
  65.5 24.5 %collective-permute-start.10 = (bf16[1,2048,256]{2,1,0:T(8,128)(2,1)}, bf16[1,2048,256]{2,1,0:T(8,128)(2,1)}, u32[]{:S(2)}, u32[]{:S(2)}) collective-permute-start(bf16[1,2048,256]{2,1,0:T(8,128)(2,1)} %collective-permute-done.9), channel_id=1, source_target_pairs={{0,1},{1,0},{2,3},{3,2},{4,5},{5,4},{6,7},{7,6},{8,9},{9,8},{10,11... | collective-permute-start | bytes 3145736 | tf_op jit(solution)/shard_map/ppermute | solution.py:15
  68.9 34.3 %collective-permute-start.11 = (bf16[1,256,2048]{2,1,0:T(8,128)(2,1)}, bf16[1,256,2048]{2,1,0:T(8,128)(2,1)}, u32[]{:S(2)}, u32[]{:S(2)}) collective-permute-start(bf16[1,256,2048]{2,1,0:T(8,128)(2,1)} %param.26), channel_id=1, source_target_pairs={{0,1},{1,0},{2,3},{3,2},{4,5},{5,4},{6,7},{7,6},{8,9},{9,8},{10,11... | collective-permute-start | bytes 3145736 | tf_op jit(solution)/shard_map/ppermute | solution.py:15
  86.1 19.9 %collective-permute-start.13 = (bf16[1,256,2048]{2,1,0:T(8,128)(2,1)S(1)}, bf16[1,256,2048]{2,1,0:T(8,128)(2,1)}, u32[]{:S(2)}, u32[]{:S(2)}) collective-permute-start(bf16[1,256,2048]{2,1,0:T(8,128)(2,1)S(1)} %collective-permute-done.12), channel_id=1, source_target_pairs={{0,1},{1,0},{2,3},{3,2},{4,5},{5,4},{6,7},{7,6},{8,9},{9,8},{10,11... | collective-permute-start | bytes 3145736 | tf_op jit(solution)/shard_map/ppermute | solution.py:15
  93.7 5.3 %copy-start.4 = (bf16[1,2048,1024]{2,1,0:T(8,128)(2,1)S(1)}, bf16[1,2048,1024]{2,1,0:T(8,128)(2,1)}, u32[]{:S(2)}) copy-start(bf16[1,2048,1024]{2,1,0:T(8,128)(2,1)} %pad_maximum_fusion.1) | copy-start | bytes 12582916
  109.9 5.9 %copy-start.7 = (f32[512,512]{1,0:T(8,128)S(1)}, f32[512,512]{1,0:T(8,128)}, u32[]{:S(2)}) copy-start(f32[512,512]{1,0:T(8,128)} %convert_multiply_fusion.4) | copy-start | bytes 3145732
  109.9 54.9 %all-to-all-start.1 = ((bf16[8,64,2048]{2,1,0:T(8,128)(2,1)}), bf16[8,64,2048]{2,1,0:T(8,128)(2,1)}, u32[]{:S(2)}, u32[]{:S(2)}) async-start(bf16[8,64,2048]{2,1,0:T(8,128)(2,1)} %bitcast.77), calls=%async_computation.1 | async-start | bytes 4194304 | tf_op jit(solution)/shard_map/all_to_all | solution.py:184
  118.2 1.4 copy-start.6
  118.2 2.6 %copy-start.10 = (bf16[256,2048]{1,0:T(8,128)(2,1)S(1)}, bf16[256,2048]{1,0:T(8,128)(2,1)}, u32[]{:S(2)}) copy-start(bf16[256,2048]{1,0:T(8,128)(2,1)} %param.29) | copy-start | bytes 3145732
  120.6 8.6 %collective-permute-start.1 = (bf16[2,128,2048]{2,1,0:T(8,128)(2,1)}, bf16[2,128,2048]{2,1,0:T(8,128)(2,1)}, u32[]{:S(2)}, u32[]{:S(2)}) collective-permute-start(bf16[2,128,2048]{2,1,0:T(8,128)(2,1)} %dynamic-slice_bitcast_fusion.1), channel_id=1, source_target_pairs={{0,1},{1,0},{2,3},{3,2},{4,5},{5,4},{6,7},{7,6},{8,9},{9,8},{10,11... | collective-permute-start | bytes 3145736 | tf_op jit(solution)/shard_map/ppermute | solution.py:15
  126.5 2.6 %copy-start.9 = (f32[512,2]{0,1:T(2,128)S(1)}, f32[512,2]{0,1:T(2,128)}, u32[]{:S(2)}) copy-start(f32[512,2]{0,1:T(2,128)} %param.23) | copy-start | bytes 12292
  128.9 4.1 %collective-permute-start.3 = (bf16[2,128,2048]{2,1,0:T(8,128)(2,1)}, bf16[2,128,2048]{2,1,0:T(8,128)(2,1)S(1)}, u32[]{:S(2)}, u32[]{:S(2)}) collective-permute-start(bf16[2,128,2048]{2,1,0:T(8,128)(2,1)} %dynamic-slice_bitcast_fusion), channel_id=1, source_target_pairs={{0,1},{1,0},{2,3},{3,2},{4,5},{5,4},{6,7},{7,6},{8,9},{9,8},{10,11... | collective-permute-start | bytes 3145736 | tf_op jit(solution)/shard_map/ppermute | solution.py:15
  129.2 3.7 %copy-start.5 = (bf16[512,2048]{1,0:T(8,128)(2,1)S(1)}, bf16[512,2048]{1,0:T(8,128)(2,1)}, u32[]{:S(2)}) copy-start(bf16[512,2048]{1,0:T(8,128)(2,1)} %convolution_convert_fusion) | copy-start | bytes 6291460
  131.4 14.9 %collective-permute-start.2 = (bf16[1,128,2048]{2,1,0:T(8,128)(2,1)S(1)}, bf16[1,128,2048]{2,1,0:T(8,128)(2,1)S(1)}, u32[]{:S(2)}, u32[]{:S(2)}) collective-permute-start(bf16[1,128,2048]{2,1,0:T(8,128)(2,1)S(1)} %dynamic-slice_convert_fusion.1), channel_id=1, source_target_pairs={{0,2},{1,3},{2,0},{3,1},{4,6},{5,7},{6,4},{7,5},{8,10},{9,11},{10,... | collective-permute-start | bytes 1572872 | tf_op jit(solution)/shard_map/ppermute | solution.py:15
  133.3 1.4 copy-start.1
  134.8 34.3 %collective-permute-start.4 = (bf16[1,128,2048]{2,1,0:T(8,128)(2,1)S(1)}, bf16[1,128,2048]{2,1,0:T(8,128)(2,1)S(1)}, u32[]{:S(2)}, u32[]{:S(2)}) collective-permute-start(bf16[1,128,2048]{2,1,0:T(8,128)(2,1)S(1)} %dynamic-slice_convert_fusion), channel_id=1, source_target_pairs={{0,2},{1,3},{2,0},{3,1},{4,6},{5,7},{6,4},{7,5},{8,10},{9,11},{10,... | collective-permute-start | bytes 1572872 | tf_op jit(solution)/shard_map/ppermute | solution.py:15
  166.8 2.2 %copy-start.2 = (f32[2,128,2048]{2,1,0:T(8,128)S(1)}, f32[2,128,2048]{2,1,0:T(8,128)}, u32[]{:S(2)}) copy-start(f32[2,128,2048]{2,1,0:T(8,128)} %copy-done.1) | copy-start | bytes 6291460
